TPU v7x, 512 devices: a whole 4x4x16 slice. The times are simulated.
512 devices in a mesh: ep: 32 (over z, core), tp: 16 (over y, x).
Axes of the slice: x: 4, y: 4, z: 16, core: 2. Of those that a mesh axis runs over, the one named last changes fastest.
Arguments:
- tokens: bfloat16 [4096, 2048], P('ep'), may hold values from -6 to 6
- selected: int32 [32, 1024], P(None, 'ep'), may hold values from -1 to 127, as said below
- affinity: float32 [32, 1024], P(None, 'ep'), may hold values from 0.05 to 1
- w_gate: bfloat16 [32, 2048, 2048], P('ep', None, 'tp'), may hold values from -0.125 to 0.125
- w_up: bfloat16 [32, 2048, 2048], P('ep', None, 'tp'), may hold values from -0.125 to 0.125
- w_down: bfloat16 [32, 2048, 2048], P('ep', 'tp'), may hold values from -0.125 to 0.125
Outputs:
- combined: bfloat16 [4096, 2048], P('ep', 'tp')
Inputs may be any that keep to these rules, and one draw needn't show every extreme that they name: `selected`: row e holds 32 aligned groups of 32 entries; the live entries of group j are distinct positions within the j-th block of 128 tokens, stand at the front of the group and are followed by -1; each row has 512 live entries in all, the number in a group varies, and some group of every row is full.
All inputs are finite; a program needn't handle non-finite values.
Results may differ from a plain program's by a relative error of at most 0.015.
Values may be sent and summed in bfloat16 or wider, within the bound.
A program may use at most 64 MiB of HBM per device.

v0:
```python
import jax
import jax.numpy as jnp
from jax import lax
from jax.sharding import Mesh
from jax.sharding import PartitionSpec as P

EP = ("ep_0", "ep_1")


def in_blocks(array, dim, peers):
    dims = array.shape
    parts = array.reshape(*dims[:dim], peers, dims[dim] // peers, *dims[dim + 1 :])
    return jnp.moveaxis(parts, dim, 0)


def joined_along(parts, dim):
    dims = list(parts.shape[1:])
    dims[dim] *= parts.shape[0]
    return jnp.moveaxis(parts, 0, dim).reshape(dims)


def moved_by_axis(parts, axes, order):
    dims = [lax.axis_size(a) for a in axes]
    parts = parts.reshape(*dims, *parts.shape[1:])
    for k in order:
        parts = lax.all_to_all(parts, axes[k], split_axis=k, concat_axis=k, tiled=True)
    return parts.reshape(-1, *parts.shape[len(axes) :])


def two_step_exchange(array, groups, order, split_dim, concat_dim):
    peers = lax.axis_size(groups[0]) * lax.axis_size(groups[1])
    parts = in_blocks(array, split_dim, peers)
    return joined_along(moved_by_axis(parts, groups, order), concat_dim)


def sent_to_all(array, axis):
    peers = lax.axis_size(axis)
    return lax.all_to_all(
        jnp.broadcast_to(array[None], (peers, *array.shape)), axis, 0, 0, tiled=True
    )


def gather_directly(array, axis, dim):
    parts = sent_to_all(array, axis)
    return joined_along(parts, dim)


def summed_on_arrival(array, axis, dim):
    peers = lax.axis_size(axis)
    parts = lax.all_to_all(in_blocks(array, dim, peers), axis, 0, 0, tiled=True)
    return jnp.sum(parts.astype(jnp.float32), axis=0)


def per_device(tokens, selected, affinity, w_gate, w_up, w_down):
    ep_count = lax.axis_size(EP)
    tp_count = lax.axis_size("tp")
    local_tokens = tokens.shape[0]
    width = tokens.shape[1]
    experts_here = w_gate.shape[0]
    slot_count = selected.shape[1]
    clamped = jnp.maximum(selected, 0)
    gathered = jnp.take(tokens, clamped, axis=0)
    column_span = width // tp_count
    slab = lax.dynamic_slice_in_dim(gathered, lax.axis_index("tp") * column_span, column_span, 2)
    arrived = two_step_exchange(slab, ("ep_0", "ep_1"), (1, 0), 0, 1)
    segment = gather_directly(arrived, "tp", 2)
    gate_more = jnp.einsum("ecd,edf->ecf", segment, w_gate, preferred_element_type=jnp.float32)
    up_more = jnp.einsum("ecd,edf->ecf", segment, w_up, preferred_element_type=jnp.float32)
    hidden = (jax.nn.silu(gate_more) * up_more).astype(jnp.bfloat16)
    summed = summed_on_arrival(
        jnp.einsum("efd,ecf->dec", w_down, hidden, preferred_element_type=jnp.float32).astype(
            jnp.bfloat16
        ),
        "tp",
        0,
    ).astype(jnp.bfloat16)
    summed = summed.reshape(summed.shape[0], experts_here, ep_count, slot_count)
    returned = lax.all_to_all(summed, EP, split_axis=2, concat_axis=1, tiled=True)
    feature_cols = returned.shape[0]
    returned = returned.reshape(feature_cols, experts_here * ep_count * slot_count)
    weights = jnp.where(selected >= 0, affinity, jnp.zeros_like(affinity)).reshape(-1)
    scaled_rows = returned.astype(jnp.float32).T * weights[:, None]
    combined = (
        jnp.zeros((local_tokens, feature_cols), jnp.float32)
        .at[clamped.reshape(-1)]
        .add(scaled_rows)
    )
    return combined.astype(jnp.bfloat16)


def solution(mesh):
    torus = Mesh(mesh.devices.reshape(16, 2, mesh.shape["tp"]), ("ep_0", "ep_1", "tp"))
    in_specs = (
        P(EP, None),
        P(None, EP),
        P(None, EP),
        P(EP, None, "tp"),
        P(EP, None, "tp"),
        P(EP, "tp", None),
    )
    out_specs = P(EP, "tp")
    return jax.shard_map(
        per_device, mesh=torus, in_specs=in_specs, out_specs=out_specs, check_vma=False
    )
```

profile of v0, /device:TPU:1, one launch (start us, length us, event | category | flops | bytes accessed | tf_op | source)
XLA Modules:
  0.0 214.1 jit_solution(5828575752059299651)
XLA Ops:
  0.0 0.0 copy-start
  0.0 0.8 broadcast_maximum_fusion
  0.8 0.7 broadcast_compare_fusion
  1.5 0.1 reshape.94
  1.6 0.0 copy-done
  1.6 6.0 %gather_fusion = bf16[1024,2048]{1,0:T(8,128)(2,1)} fusion(bf16[128,2048]{1,0:T(8,128)(2,1)S(1)} %copy-done, s32[1024]{0:T(1024)S(1)} %broadcast_clamp_fusion), kind=kCustom, calls=%fused_computation | custom fusion | bytes 8392704 | tf_op jit(solution)/shard_map/jit(_take)/gather | solution.py:62
  7.6 1.1 dynamic-slice_select_fusion
  8.8 10.4 %all_to_all.29 = bf16[16,2,1,32,128]{4,3,0,2,1:T(8,128)(2,1)S(1)} all-to-all(bf16[16,2,1,32,128]{4,3,0,2,1:T(8,128)(2,1)S(1)} %copy.8), channel_id=1, replica_groups=mesh['ep_0'=16,'ep_1'=2,'tp'=16] {'ep_1'}, dimensions={1} | all-to-all | bytes 524288 | tf_op jit(solution)/shard_map/all_to_all | solution.py:26
  19.2 23.4 %all_to_all.30 = bf16[16,2,1,32,128]{4,3,1,2,0:T(8,128)(2,1)S(1)} all-to-all(bf16[16,2,1,32,128]{4,3,1,2,0:T(8,128)(2,1)S(1)} %copy.9), channel_id=1, replica_groups=mesh['ep_0'=16,'ep_1'=2,'tp'=16] {'ep_0'}, dimensions={0} | all-to-all | bytes 524288 | tf_op jit(solution)/shard_map/all_to_all | solution.py:26
  42.6 0.1 copy.10
  42.7 0.5 broadcast_in_dim.31
  43.3 0.0 copy-start.2
  43.3 53.3 %all_to_all.31 = bf16[16,1,1024,128]{2,3,1,0:T(8,128)(2,1)S(1)} all-to-all(bf16[16,1,1024,128]{2,3,1,0:T(8,128)(2,1)S(1)} %broadcast_in_dim.31), channel_id=1, replica_groups=mesh['ep_0'=16,'ep_1'=2,'tp'=16] {'tp'}, dimensions={0} | all-to-all | bytes 8388608 | tf_op jit(solution)/shard_map/all_to_all | solution.py:38
  96.6 0.0 copy-start.1
  96.6 0.0 copy-start.3
  96.6 0.0 copy-start.4
  96.6 1.9 copy-done.1
  98.6 0.0 copy-done.2
  98.6 1.3 fusion.7
  99.8 0.0 copy-done.3
  99.8 0.0 copy-done.4
  99.9 8.5 %convert_bitcast_fusion = bf16[1,128,16,8,128]{4,3,2,1,0:T(8,128)(2,1)} fusion(bf16[1024,2048]{0,1:T(8,128)(2,1)} %bitcast.36, bf16[1,128,2048]{2,1,0:T(8,128)(2,1)S(1)} %copy-done.3, bf16[1,2048,128]{2,1,0:T(8,128)(2,1)S(1)} %copy-done.4, f32[1024,128]{1,0:T(8,128)S(1)} %fusion.7), kind=kOutput, calls=%fused_computation.3 | convolution fusion | flops 1076625408 | bytes 9961472 | tf_op jit(solution)/shard_map/efd,ecf->dec/dot_general | solution.py:71
  108.4 3.3 %copy.15 = bf16[1,128,16,8,128]{4,3,1,0,2:T(8,128)(2,1)S(1)} copy(bf16[1,128,16,8,128]{4,3,2,1,0:T(8,128)(2,1)} %convert_bitcast_fusion) | data formatting | bytes 8388608 | tf_op jit(solution)/shard_map/reshape | solution.py:12
  111.6 47.9 %all_to_all.32 = bf16[16,128,1,1024]{1,3,2,0:T(8,128)(2,1)} all-to-all(bf16[16,128,1,1024]{1,3,2,0:T(8,128)(2,1)S(1)} %bitcast.37), channel_id=1, replica_groups=mesh['ep_0'=16,'ep_1'=2,'tp'=16] {'tp'}, dimensions={0} | all-to-all | bytes 8388608 | tf_op jit(solution)/shard_map/all_to_all | solution.py:50
  159.6 0.0 copy-start.5
  159.6 0.0 copy-start.6
  159.6 3.5 %reduce_sum.12 = bf16[128,1024]{0,1:T(8,128)(2,1)} reduce(bf16[16,128,1,1024]{1,3,2,0:T(8,128)(2,1)} %all_to_all.32, bf16[]{:T(256)} %constant.37.clone.1), dimensions={0,2}, to_apply=%region_0.1 | reduce | flops 1966080 | bytes 4456450 | tf_op jit(solution)/shard_map/reduce_sum | solution.py:51
  163.1 21.3 %all-to-all-start.4 = ((bf16[128,1,32,32]{0,3,1,2:T(8,128)(2,1)}), bf16[128,1,32,32]{0,3,1,2:T(8,128)(2,1)S(1)}, u32[]{:S(2)}, u32[]{:S(2)}) async-start(bf16[128,1,32,32]{0,3,1,2:T(8,128)(2,1)} %bitcast.14), calls=%async_computation.4 | async-start | bytes 524288 | tf_op jit(solution)/shard_map/all_to_all | solution.py:78
  184.5 0.1 reshape.84
  184.5 0.0 copy-done.5
  184.5 0.0 copy-done.6
  184.6 0.1 mul.28
  184.6 22.1 %all-to-all-done.4 = bf16[128,1,32,32]{0,3,1,2:T(8,128)(2,1)S(1)} async-done(((bf16[128,1,32,32]{0,3,1,2:T(8,128)(2,1)}), bf16[128,1,32,32]{0,3,1,2:T(8,128)(2,1)S(1)}, u32[]{:S(2)}, u32[]{:S(2)}) %all-to-all-start.4) | async-done | bytes 262176 | tf_op jit(solution)/shard_map/all_to_all | solution.py:78
  206.7 6.8 %scatter_custom_fusion = f32[128,128]{1,0:T(8,128)S(1)} fusion(s32[1024]{0:T(1024)S(1)} %bitcast.42, bf16[128,1024]{0,1:T(8,128)(2,1)S(1)} %bitcast.40, f32[1024]{0:T(1024)S(1)} %mul.28, f32[]{:T(128)} %constant.11.clone.1), kind=kCustom, calls=%fused_computation.8 | custom fusion | flops 393216 | bytes 331780 | tf_op jit(solution)/shard_map/scatter-add | solution.py:86
  213.5 0.6 convert_element_type.30
  (5 shorter events, 0.1 us)
Async XLA Ops:
  0.0 1.6 copy-start
  43.3 55.3 %copy-start.2 = (bf16[1,2048,128]{2,1,0:T(8,128)(2,1)S(1)}, bf16[1,2048,128]{2,1,0:T(8,128)(2,1)}, u32[]{:S(2)}) copy-start(bf16[1,2048,128]{2,1,0:T(8,128)(2,1)} %param.9) | copy-start | bytes 1572868
  96.6 1.9 copy-start.1
  96.6 3.2 %copy-start.3 = (bf16[1,128,2048]{2,1,0:T(8,128)(2,1)S(1)}, bf16[1,128,2048]{2,1,0:T(8,128)(2,1)}, u32[]{:S(2)}) copy-start(bf16[1,128,2048]{2,1,0:T(8,128)(2,1)} %param.11) | copy-start | bytes 1572868
  96.6 3.2 %copy-start.4 = (bf16[1,2048,128]{2,1,0:T(8,128)(2,1)S(1)}, bf16[1,2048,128]{2,1,0:T(8,128)(2,1)}, u32[]{:S(2)}) copy-start(bf16[1,2048,128]{2,1,0:T(8,128)(2,1)} %param.10) | copy-start | bytes 1572868
  159.6 25.0 %copy-start.5 = (s32[32,32]{1,0:T(8,128)S(1)}, s32[32,32]{1,0:T(8,128)}, u32[]{:S(2)}) copy-start(s32[32,32]{1,0:T(8,128)} %param.7) | copy-start | bytes 12292
  159.6 25.0 %copy-start.6 = (f32[32,32]{1,0:T(8,128)S(1)}, f32[32,32]{1,0:T(8,128)}, u32[]{:S(2)}) copy-start(f32[32,32]{1,0:T(8,128)} %param.8) | copy-start | bytes 12292
  163.1 43.6 %all-to-all-start.4 = ((bf16[128,1,32,32]{0,3,1,2:T(8,128)(2,1)}), bf16[128,1,32,32]{0,3,1,2:T(8,128)(2,1)S(1)}, u32[]{:S(2)}, u32[]{:S(2)}) async-start(bf16[128,1,32,32]{0,3,1,2:T(8,128)(2,1)} %bitcast.14), calls=%async_computation.4 | async-start | bytes 524288 | tf_op jit(solution)/shard_map/all_to_all | solution.py:78
where the time goes:
time: 215 us; the launch traced here: 214 us
  blocking collectives  135 us (63%)
  waiting for transfers between devices  22.1 us (10%)
  starting transfers between devices  21.3 us (10%)
  other arithmetic  13.6 us (6%)
  local copies, waits for them, and re-layouts  12.1 us (6%)
  matrix products  9.8 us (5%)
    all_to_all x1, blocking collectives, sent_to_all(): lax.all_to_all(jnp.broadcast_to(array[None], (peers, *array.shape)), axis...  53.3 us
    all_to_all x1, blocking collectives, summed_on_arrival(): parts = lax.all_to_all(in_blocks(array, dim, peers), axis, 0, 0, tiled=True)  47.9 us
    all_to_all x2, blocking collectives, moved_by_axis(): lax.all_to_all(parts, axes[k], split_axis=k, concat_axis=k, tiled=True)  33.8 us
    all_to_all x1, waiting for transfers between devices, per_device(): lax.all_to_all(summed, EP, split_axis=2, concat_axis=1, tiled=True)  22.1 us
    all_to_all x1, starting transfers between devices, per_device(): lax.all_to_all(summed, EP, split_axis=2, concat_axis=1, tiled=True)  21.3 us
    dot_general x1, matrix products, per_device(): jnp.einsum('efd,ecf->dec', w_down, hidden, preferred_element_type=jnp.flo...  8.52 us
    scatter-add x1, other arithmetic, per_device(): combined = jnp.zeros((local_tokens, feature_cols), jnp.float32).at[clampe...  6.81 us
    gather x1, local copies, waits for them, and re-layouts, per_device(): gathered = jnp.take(tokens, clamped, axis=0)  5.98 us
  transfers between devices with their start and end apart: 1, of which 1 were waited for; matrix products, arithmetic and copies ran while one was open for 0% of the time, Pallas kernels for 0%

commit v1 on v0

v1 whole, which is shorter than its diff:
```python
import functools

import jax
import jax.numpy as jnp
from jax import lax
from jax.experimental import pallas as pl
from jax.experimental.pallas import tpu as pltpu
from jax.sharding import PartitionSpec as P

MESH = pl.DeviceIdType.MESH
BF = jnp.bfloat16
F32 = jnp.float32

N_EP, N_TP, N_Z, SIDE = 32, 16, 16, 4
MOST, TOK, WID = 32, 128, 128
ROWS, CHUNK = 512, 128
CHUNKS = ROWS // CHUNK
HALF = CHUNK // 2
PER = CHUNK // MOST
EARLY = N_EP - PER * (CHUNKS - 1)
DEAD = 1024.0

PLACES = [(0, 0), (0, 1)]
for _d in range(1, N_Z // 2):
    PLACES += [(_d, 0), (_d, 1), (N_Z - _d, 0), (N_Z - _d, 1)]
PLACES += [(N_Z // 2, 0), (N_Z // 2, 1)]
SUM_ORDER = (0, 3, 2, 1)


def remote(src, dst, send, recv, device):
    return pltpu.make_async_remote_copy(
        src_ref=src, dst_ref=dst, send_sem=send, recv_sem=recv, device_id=device, device_id_type=MESH
    )


def kernel(
    tok, sel, aff, wg, wu, wd, out,
    tokb, selb, affb, wgu, wdb, onehot, sent, came, pick, spread, rows, part, got1, sum1, got2,
    result, back, home, mix,
    in_sem, z_send, z_recv, a1_send, a1_recv, a2_send, a2_recv,
    r1_send, r1_recv, r2_send, r2_recv, b_send, b_recv,
):
    ep, tp = lax.axis_index("ep"), lax.axis_index("tp")
    z, core = ep // 2, ep % 2
    y, x = tp // SIDE, tp % SIDE

    def ep_peer(i):
        dz, dc = PLACES[i]
        e = lax.rem(z + dz, N_Z) * 2 + lax.rem(core + dc, 2)
        return e, {"ep": e, "tp": tp}

    def ep_back(i):
        dz, dc = PLACES[i]
        e = lax.rem(z + N_Z - dz, N_Z) * 2 + lax.rem(core + dc, 2)
        return e, {"ep": e, "tp": tp}

    def line(axis, i):
        if axis == 0:
            t = y * SIDE + lax.rem(x + i, SIDE)
        else:
            t = lax.rem(y + i, SIDE) * SIDE + x
        return t, {"ep": ep, "tp": t}

    loads = [
        pltpu.make_async_copy(sel, selb, in_sem.at[0]),
        pltpu.make_async_copy(aff, affb, in_sem.at[1]),
        pltpu.make_async_copy(
            tok.at[:, pl.ds(pl.multiple_of(tp * WID, WID), WID)], tokb.at[pl.ds(0, TOK)], in_sem.at[2]
        ),
        pltpu.make_async_copy(wg, wgu.at[:, pl.ds(0, WID)], in_sem.at[3]),
        pltpu.make_async_copy(wu, wgu.at[:, pl.ds(WID, WID)], in_sem.at[4]),
        pltpu.make_async_copy(wd, wdb, in_sem.at[5]),
    ]
    for load in loads:
        load.start()
    barrier = pltpu.get_barrier_semaphore()
    peers = [ep_peer(i)[1] for i in range(1, N_EP)]
    peers += [line(a, i)[1] for a in (0, 1) for i in (1, 2, 3)]
    for peer in peers:
        pl.semaphore_signal(barrier, inc=1, device_id=peer, device_id_type=MESH)

    tokb[TOK : 2 * TOK] = jnp.full((TOK, WID), DEAD, BF)
    loads[0].wait()
    loads[1].wait()
    sel_t = selb[...].astype(F32).T
    aff_t = affb[...].T
    lane2 = lax.broadcasted_iota(jnp.int32, (MOST, 2 * TOK), 1).astype(F32)
    lane1 = lax.broadcasted_iota(jnp.int32, (MOST, TOK), 1).astype(F32)
    for e in range(N_EP):
        column = sel_t[:, e : e + 1]
        spot = jnp.where(column < 0.0, float(TOK), column)
        onehot[e * MOST : (e + 1) * MOST] = jnp.where(lane2 == spot, 1.0, 0.0).astype(BF)
    loads[2].wait()
    sent[...] = (
        jnp.dot(onehot[...], tokb[...], preferred_element_type=F32).astype(BF).reshape(N_EP, MOST, WID)
    )
    came[0] = sent[ep]
    pl.semaphore_wait(barrier, len(peers))

    zs = []
    for i in range(1, N_EP):
        e, peer = ep_peer(i)
        copy = remote(sent.at[e], came.at[i], z_send.at[i], z_recv.at[i], peer)
        copy.start()
        zs.append(copy)

    for q in range(N_EP * MOST // TOK):
        tall = []
        for e in range(q * PER, (q + 1) * PER):
            tall.append(jnp.where(lane1 == sel_t[:, e : e + 1], aff_t[:, e : e + 1], 0.0))
        wide = jnp.concatenate(tall, axis=0).T
        high = wide.astype(BF)
        mix[0, :, q * TOK : (q + 1) * TOK] = high
        mix[1, :, q * TOK : (q + 1) * TOK] = (wide - high.astype(F32)).astype(BF)

    lane_row = lax.broadcasted_iota(jnp.int32, (1, WID), 1)
    lane_slot = lax.rem(lane_row, MOST).astype(F32)
    lane_group = lane_row // MOST
    down_rows = lax.broadcasted_iota(jnp.int32, (CHUNK, WID), 0).astype(F32)

    starts, counts = [], []
    total = jnp.zeros((1, WID), F32)
    copies = {"a1": {}, "a2": {}, "r1": {}, "r2": {}}

    def span(c, half):
        return pl.ds(c * CHUNK + half * HALF, HALF)

    def begin_gather(c):
        for i in (2, 1, 3):
            for half in (0, 1):
                block = rows.at[tp, span(c, half)]
                copy = remote(
                    block, block, a1_send.at[c, half, i], a1_recv.at[c, half, i], line(half, i)[1]
                )
                copy.start()
                copies["a1"][c, half, i] = copy
        for i in (2, 1, 3):
            for half in (0, 1):
                block = rows.at[tp, span(c, half)]
                copy = remote(
                    block, block, a2_send.at[c, half, i, 0], a2_recv.at[c, half, i, 0], line(1 - half, i)[1]
                )
                copy.start()
                copies["a2"][c, half, i, 0] = copy

    def pass_on(c):
        for j in (1, 3, 2):
            for half in (0, 1):
                copies["a1"][c, half, j].wait_recv()
                source = line(half, SIDE - j)[0]
                block = rows.at[source, span(c, half)]
                for i in (2, 1, 3):
                    copy = remote(
                        block, block, a2_send.at[c, half, i, j], a2_recv.at[c, half, i, j], line(1 - half, i)[1]
                    )
                    copy.start()
                    copies["a2"][c, half, i, j] = copy

    for c in range(CHUNKS):
        known = EARLY + PER * c
        for j in range(len(counts), known):
            if j > 0:
                zs[j - 1].wait_recv()
        for j in range(len(counts), known):
            live = jnp.where(came[j].astype(F32) < DEAD / 2, 1.0, 0.0)
            n = jnp.sum(live, axis=0, keepdims=True)
            counts.append(n)
            starts.append(total)
            total = total + n
        for t in range(EARLY // PER):
            g = (c + t) * PER
            first, many = starts[g + PER - 1], counts[g + PER - 1]
            for k in range(PER - 2, -1, -1):
                first = jnp.where(lane_group == k, starts[g + k], first)
                many = jnp.where(lane_group == k, counts[g + k], many)
            place = jnp.where(lane_slot < many, first + lane_slot, -1.0)
            pick[:, t * WID : (t + 1) * WID] = jnp.where(
                down_rows + float(c * CHUNK) == place, 1.0, 0.0
            ).astype(BF)
        block = came[PER * c : PER * c + EARLY].reshape(EARLY * MOST, WID)
        rows[tp, c * CHUNK : (c + 1) * CHUNK] = jnp.dot(
            pick[...], block, preferred_element_type=F32
        ).astype(BF)
        begin_gather(c)
        if c > 0:
            pass_on(c - 1)
    pass_on(CHUNKS - 1)

    down_slots = lax.broadcasted_iota(jnp.int32, (MOST, WID), 0).astype(F32)
    lanes = lax.broadcasted_iota(jnp.int32, (MOST, WID), 1).astype(F32)
    for j in range(N_EP):
        place = jnp.where(down_slots < counts[j], starts[j] + down_slots, -1.0)
        for c in range(CHUNKS):
            spread[j * MOST : (j + 1) * MOST, c * WID : (c + 1) * WID] = jnp.where(
                lanes + float(c * CHUNK) == place, 1.0, 0.0
            ).astype(BF)
    for load in loads[3:]:
        load.wait()

    def compute(c):
        for half in (0, 1):
            for i in (1, 2, 3):
                for j in range(SIDE):
                    copies["a2"][c, half, i, j].wait_recv()
        at = slice(c * CHUNK, (c + 1) * CHUNK)
        chosen = jnp.concatenate([rows[k, at] for k in range(N_TP)], axis=1)
        both = jnp.dot(chosen, wgu[...], preferred_element_type=F32)
        gate, up = both[:, :WID], both[:, WID:]
        hidden = (gate / (1.0 + jnp.exp(-gate)) * up).astype(BF)
        partial = jnp.dot(hidden, wdb[...], preferred_element_type=F32).astype(BF)
        for k in range(N_TP):
            part[k // SIDE, k % SIDE, at] = partial[:, k * WID : (k + 1) * WID]

    def begin_sum(c):
        for i in (2, 1, 3):
            for half in (0, 1):
                t, peer = line(half, i)
                if half == 0:
                    block = part.at[:, t % SIDE, span(c, half)]
                else:
                    block = part.at[t // SIDE, :, span(c, half)]
                copy = remote(
                    block, got1.at[c, half, i - 1], r1_send.at[c, half, i], r1_recv.at[c, half, i], peer
                )
                copy.start()
                copies["r1"][c, half, i] = copy

    def go_on_sum(c):
        for half in (0, 1):
            for i in (1, 3, 2):
                copies["r1"][c, half, i].wait_recv()
            mine = part[:, x, span(c, half)] if half == 0 else part[y, :, span(c, half)]
            added = mine.astype(F32)
            for i in range(3):
                added = added + got1[c, half, i].astype(F32)
            sum1[c, half] = added.astype(BF)
            for i in (2, 1, 3):
                t, peer = line(1 - half, i)
                block = sum1.at[c, half, t // SIDE if half == 0 else t % SIDE]
                copy = remote(
                    block, got2.at[c, half, i - 1], r2_send.at[c, half, i], r2_recv.at[c, half, i], peer
                )
                copy.start()
                copies["r2"][c, half, i] = copy

    def end_sum(c):
        for half in (0, 1):
            for i in (1, 3, 2):
                copies["r2"][c, half, i].wait_recv()
            added = sum1[c, half, y if half == 0 else x].astype(F32)
            for i in range(3):
                added = added + got2[c, half, i].astype(F32)
            result[span(c, half)] = added.astype(BF)

    bs = {}

    def give_back(first, last):
        low = (min(first // PER, CHUNKS - 1) if first >= EARLY else 0) if first else 0
        low = max(0, (first - EARLY) // PER + 1) if first >= EARLY else 0
        slots = jnp.dot(
            spread[first * MOST : last * MOST, low * WID :], result[low * CHUNK :], preferred_element_type=F32
        ).astype(BF)
        back[first:last] = slots.reshape(last - first, MOST, WID)
        for i in range(last - 1, first - 1, -1):
            if i == 0:
                home[ep] = back[0]
                continue
            peer = ep_back(i)[1]
            copy = remote(back.at[i], home.at[ep], b_send.at[i], b_recv.at[i], peer)
            copy.start()
            bs[i] = copy

    for c in range(CHUNKS):
        compute(c)
        if c == 0:
            begin_sum(0)
    for c in SUM_ORDER[1:]:
        begin_sum(c)
    done, left = set(), N_EP
    for n, c in enumerate(SUM_ORDER):
        go_on_sum(c)
        if n > 0:
            before = SUM_ORDER[n - 1]
            end_sum(before)
            done.add(before)
            first = left
            while first > EARLY and all(k in done for k in range((first - 1 - EARLY) // PER + 1, CHUNKS)):
                first -= PER
            if first < left:
                give_back(first, left)
                left = first
    end_sum(SUM_ORDER[-1])
    give_back(0, left)

    for i in range(1, N_EP):
        bs[i].wait_recv()
    slots = home[...].reshape(N_EP * MOST, WID)
    out[...] = (
        jnp.dot(mix[0], slots, preferred_element_type=F32) + jnp.dot(mix[1], slots, preferred_element_type=F32)
    ).astype(BF)
    for copy in zs:
        copy.wait_send()
    for group in copies.values():
        for copy in group.values():
            copy.wait_send()
    for copy in bs.values():
        copy.wait_send()


def per_device(tokens, selected, affinity, w_gate, w_up, w_down):
    width = tokens.shape[1]
    dma = pltpu.SemaphoreType.DMA
    scratch = [
        pltpu.VMEM((2 * TOK, WID), BF),
        pltpu.VMEM((N_EP, MOST), jnp.int32),
        pltpu.VMEM((N_EP, MOST), F32),
        pltpu.VMEM((width, 2 * WID), BF),
        pltpu.VMEM((WID, width), BF),
        pltpu.VMEM((N_EP * MOST, 2 * TOK), BF),
        pltpu.VMEM((N_EP, MOST, WID), BF),
        pltpu.VMEM((N_EP, MOST, WID), BF),
        pltpu.VMEM((CHUNK, EARLY * MOST), BF),
        pltpu.VMEM((N_EP * MOST, ROWS), BF),
        pltpu.VMEM((N_TP, ROWS, WID), BF),
        pltpu.VMEM((SIDE, SIDE, ROWS, WID), BF),
        pltpu.VMEM((CHUNKS, 2, 3, SIDE, HALF, WID), BF),
        pltpu.VMEM((CHUNKS, 2, SIDE, HALF, WID), BF),
        pltpu.VMEM((CHUNKS, 2, 3, HALF, WID), BF),
        pltpu.VMEM((ROWS, WID), BF),
        pltpu.VMEM((N_EP, MOST, WID), BF),
        pltpu.VMEM((N_EP, MOST, WID), BF),
        pltpu.VMEM((2, TOK, N_EP * MOST), BF),
        dma((6,)),
        dma((N_EP,)),
        dma((N_EP,)),
        dma((CHUNKS, 2, 4)),
        dma((CHUNKS, 2, 4)),
        dma((CHUNKS, 2, 4, 4)),
        dma((CHUNKS, 2, 4, 4)),
        dma((CHUNKS, 2, 4)),
        dma((CHUNKS, 2, 4)),
        dma((CHUNKS, 2, 4)),
        dma((CHUNKS, 2, 4)),
        dma((N_EP,)),
        dma((N_EP,)),
    ]
    return pl.pallas_call(
        kernel,
        out_shape=jax.ShapeDtypeStruct((tokens.shape[0], WID), BF),
        in_specs=[pl.BlockSpec(memory_space=pl.ANY)] * 6,
        out_specs=pl.BlockSpec(memory_space=pltpu.VMEM),
        scratch_shapes=scratch,
        compiler_params=pltpu.CompilerParams(
            collective_id=0, has_side_effects=True, vmem_limit_bytes=48 * 1024 * 1024
        ),
    )(tokens, selected, affinity, w_gate[0], w_up[0], w_down[0])


def solution(mesh):
    return jax.shard_map(
        per_device,
        mesh=mesh,
        in_specs=(
            P("ep", None),
            P(None, "ep"),
            P(None, "ep"),
            P("ep", None, "tp"),
            P("ep", None, "tp"),
            P("ep", "tp", None),
        ),
        out_specs=P("ep", "tp"),
        check_vma=False,
    )
```

time: 215 us -> 87.8 us (0.41)
  blocking collectives: 135 us -> 0 us
  Pallas kernels: 0 us -> 81.2 us
  waiting for transfers between devices: 22.1 us -> 0 us
  starting transfers between devices: 21.3 us -> 0 us
  other arithmetic: 13.6 us -> 0 us
  matrix products: 9.8 us -> 0 us
  local copies, waits for them, and re-layouts: 12.1 us -> 6.22 us
    all_to_all x4 -> x0, blocking collectives: 135 us -> none  [the longest x1 53.3 us: sent_to_all(): lax.all_to_all(jnp.broadcast_to(array[None], (peers, *array.shape)), axis...]
    pallas_call x0 -> x1, Pallas kernels: none -> 81.2 us  [per_device(): pl.pallas_call(kernel, out_shape=jax.ShapeDtypeStruct((tokens.shape[0], W...]
    all_to_all x1 -> x0, waiting for transfers between devices: 22.1 us -> none  [per_device(): lax.all_to_all(summed, EP, split_axis=2, concat_axis=1, tiled=True)]
    all_to_all x1 -> x0, starting transfers between devices: 21.3 us -> none  [per_device(): lax.all_to_all(summed, EP, split_axis=2, concat_axis=1, tiled=True)]
    dot_general x2 -> x0, matrix products: 9.8 us -> none  [the longest x1 8.52 us: per_device(): jnp.einsum('efd,ecf->dec', w_down, hidden, preferred_element_type=jnp.flo...]
    scatter-add x1 -> x0, other arithmetic: 6.81 us -> none  [per_device(): combined = jnp.zeros((local_tokens, feature_cols), jnp.float32).at[clampe...]
    gather x1 -> x0, local copies, waits for them, and re-layouts: 5.98 us -> none  [per_device(): gathered = jnp.take(tokens, clamped, axis=0)]
    unnamed x14 -> x13, local copies, waits for them, and re-layouts: 1.96 us -> 6.22 us
  transfers between devices with their start and end apart: 1 -> 0, of which waited for: 1 -> 0; matrix products, arithmetic and copies ran while one was open for 0% -> 0% of each run, Pallas kernels for 0% -> 0%
where the time goes in v1:
time: 87.8 us; the launch traced here: 87.4 us
  Pallas kernels  81.2 us (92%)
  local copies, waits for them, and re-layouts  6.22 us (7%)
    pallas_call x1, Pallas kernels, per_device(): pl.pallas_call(kernel, out_shape=jax.ShapeDtypeStruct((tokens.shape[0], W...  81.2 us
    unnamed x13, local copies, waits for them, and re-layouts  6.22 us

profile of v1, /device:TPU:1, one launch (start us, length us, event | category | flops | bytes accessed | tf_op | source)
XLA Modules:
  0.0 87.4 jit_solution(16001349933714592422)
XLA Ops:
  0.0 0.0 copy-start
  0.0 1.0 %copy-done = bf16[128,2048]{1,0:T(8,128)(2,1)S(1)} copy-done((bf16[128,2048]{1,0:T(8,128)(2,1)S(1)}, bf16[128,2048]{1,0:T(8,128)(2,1)}, u32[]{:S(2)}) %copy-start) | copy-done | bytes 524312
  1.0 0.0 copy-start.1
  1.0 1.0 %copy-done.1 = bf16[1,2048,128]{2,1,0:T(8,128)(2,1)S(1)} copy-done((bf16[1,2048,128]{2,1,0:T(8,128)(2,1)S(1)}, bf16[1,2048,128]{2,1,0:T(8,128)(2,1)}, u32[]{:S(2)}) %copy-start.1) | copy-done | bytes 524312
  2.1 0.0 copy-start.2
  2.1 1.0 %copy-done.2 = bf16[1,2048,128]{2,1,0:T(8,128)(2,1)S(1)} copy-done((bf16[1,2048,128]{2,1,0:T(8,128)(2,1)S(1)}, bf16[1,2048,128]{2,1,0:T(8,128)(2,1)}, u32[]{:S(2)}) %copy-start.2) | copy-done | bytes 524312
  3.1 0.0 copy-start.3
  3.1 1.0 %copy-done.3 = bf16[1,128,2048]{2,1,0:T(8,128)(2,1)S(1)} copy-done((bf16[1,128,2048]{2,1,0:T(8,128)(2,1)S(1)}, bf16[1,128,2048]{2,1,0:T(8,128)(2,1)}, u32[]{:S(2)}) %copy-start.3) | copy-done | bytes 524312
  4.2 0.0 copy-start.4
  4.2 0.7 copy-done.4
  4.9 0.0 copy-start.5
  4.9 0.7 copy-done.5
  5.6 81.2 %shard_map.64 = bf16[128,128]{1,0:T(8,128)(2,1)S(1)} custom-call(bf16[128,2048]{1,0:T(8,128)(2,1)S(1)} %copy-done, s32[32,32]{1,0:T(8,128)S(1)} %copy-done.4, f32[32,32]{1,0:T(8,128)S(1)} %copy-done.5, bf16[2048,128]{1,0:T(8,128)(2,1)S(1)} %bitcast.3, bf16[2048,128]{1,0:T(8,128)(2,1)S(1)} %bitcast.4, bf16[128,2048]{1,0:T(8,128)(2,1)S(1)} %bitcast.5), custom_call_target="tpu_custom_call" | custom-call | tf_op jit(solution)/shard_map/pallas_call | solution.py:347
  86.8 0.6 copy.8
Async XLA Ops:
  0.0 1.0 %copy-start = (bf16[128,2048]{1,0:T(8,128)(2,1)S(1)}, bf16[128,2048]{1,0:T(8,128)(2,1)}, u32[]{:S(2)}) copy-start(bf16[128,2048]{1,0:T(8,128)(2,1)} %tok.1) | copy-start | bytes 1572868
  1.0 1.0 %copy-start.1 = (bf16[1,2048,128]{2,1,0:T(8,128)(2,1)S(1)}, bf16[1,2048,128]{2,1,0:T(8,128)(2,1)}, u32[]{:S(2)}) copy-start(bf16[1,2048,128]{2,1,0:T(8,128)(2,1)} %param.9) | copy-start | bytes 1572868
  2.1 1.0 %copy-start.2 = (bf16[1,2048,128]{2,1,0:T(8,128)(2,1)S(1)}, bf16[1,2048,128]{2,1,0:T(8,128)(2,1)}, u32[]{:S(2)}) copy-start(bf16[1,2048,128]{2,1,0:T(8,128)(2,1)} %param.10) | copy-start | bytes 1572868
  3.1 1.0 %copy-start.3 = (bf16[1,128,2048]{2,1,0:T(8,128)(2,1)S(1)}, bf16[1,128,2048]{2,1,0:T(8,128)(2,1)}, u32[]{:S(2)}) copy-start(bf16[1,128,2048]{2,1,0:T(8,128)(2,1)} %param.11) | copy-start | bytes 1572868
  4.2 0.7 copy-start.4
  4.9 0.7 copy-start.5

commit v2 on v1

v2 whole, which is shorter than its diff:
```python
import functools

import jax
import jax.numpy as jnp
from jax import lax
from jax.experimental import pallas as pl
from jax.experimental.pallas import tpu as pltpu
from jax.sharding import PartitionSpec as P

MESH = pl.DeviceIdType.MESH
BF = jnp.bfloat16
F32 = jnp.float32

N_EP, N_TP, N_Z, SIDE = 32, 16, 16, 4
MOST, TOK, WID = 32, 128, 128
ROWS = 512
EDGES = (0, 64, 192, 320, 448, 512)
CHUNKS = len(EDGES) - 1
LARGEST = 128
PER = WID // MOST
FULL = ROWS // MOST
TILES = 5
PAD = 2
DEAD = 1024.0

PLACES = [(0, 0), (0, 1)]
for _d in range(1, N_Z // 2):
    PLACES += [(_d, 0), (_d, 1), (N_Z - _d, 0), (N_Z - _d, 1)]
PLACES += [(N_Z // 2, 0), (N_Z // 2, 1)]
STEPS = ("Z0", "Z1", "F0", "Z2", "F1", "Z3", "F2", "Z4", "F3", "F4", "K0", "B0", "K1", "P", "K2", "K3", "K4", "B4", "S0", "B3", "S4", "B2", "S3", "E4", "B1", "S2", "E3", "S1", "E2", "E0", "E1")


def known_at(c):
    return N_EP - FULL + EDGES[c + 1] // MOST


def stage_of(i):
    return next(c for c in range(CHUNKS) if i < known_at(c))


def chunks_of(i):
    return [c for c in range(CHUNKS) if EDGES[c] // MOST <= i < known_at(c)]


def remote(src, dst, send, recv, device):
    return pltpu.make_async_remote_copy(
        src_ref=src, dst_ref=dst, send_sem=send, recv_sem=recv, device_id=device, device_id_type=MESH
    )


def kernel(
    tok, sel, aff, wg, wu, wd, out,
    tokb, selb, affb, wgu, wdb, onehot, sent, came, pick, spread, rows, part, got1, sum1, got2,
    result, back, home, mix,
    chain, in_sem, z_send, z_recv, a1_send, a1_recv, a2_send, a2_recv,
    r1_send, r1_recv, r2_send, r2_recv, b_send, b_recv,
):
    ep, tp = lax.axis_index("ep"), lax.axis_index("tp")
    z, core = ep // 2, ep % 2
    y, x = tp // SIDE, tp % SIDE

    def ep_peer(i):
        dz, dc = PLACES[i]
        e = lax.rem(z + dz, N_Z) * 2 + lax.rem(core + dc, 2)
        return e, {"ep": e, "tp": tp}

    def ep_back(i):
        dz, dc = PLACES[i]
        e = lax.rem(z + N_Z - dz, N_Z) * 2 + lax.rem(core + dc, 2)
        return e, {"ep": e, "tp": tp}

    def line(axis, i):
        if axis == 0:
            t = y * SIDE + lax.rem(x + i, SIDE)
        else:
            t = lax.rem(y + i, SIDE) * SIDE + x
        return t, {"ep": ep, "tp": t}

    loads = [
        pltpu.make_async_copy(sel, selb, in_sem.at[0]),
        pltpu.make_async_copy(aff, affb, in_sem.at[1]),
        pltpu.make_async_copy(
            tok.at[:, pl.ds(pl.multiple_of(tp * WID, WID), WID)], tokb.at[pl.ds(0, TOK)], in_sem.at[2]
        ),
        pltpu.make_async_copy(wg, wgu.at[:, pl.ds(0, WID)], in_sem.at[3]),
        pltpu.make_async_copy(wu, wgu.at[:, pl.ds(WID, WID)], in_sem.at[4]),
        pltpu.make_async_copy(wd, wdb, in_sem.at[5]),
    ]
    for load in loads:
        load.start()
    barrier = pltpu.get_barrier_semaphore()
    peers = [ep_peer(i)[1] for i in range(1, 6)]
    peers += [line(a, i)[1] for a in (0, 1) for i in (1, 2, 3)]
    for peer in peers:
        pl.semaphore_signal(barrier, inc=1, device_id=peer, device_id_type=MESH)

    tokb[TOK : 2 * TOK] = jnp.full((TOK, WID), DEAD, BF)
    loads[0].wait()
    loads[1].wait()
    sel_t = selb[...].astype(F32).T
    aff_t = affb[...].T
    lane2 = lax.broadcasted_iota(jnp.int32, (MOST, 2 * TOK), 1).astype(F32)
    lane1 = lax.broadcasted_iota(jnp.int32, (MOST, TOK), 1).astype(F32)
    for e in range(N_EP):
        column = sel_t[:, e : e + 1]
        spot = jnp.where(column < 0.0, float(TOK), column)
        onehot[e * MOST : (e + 1) * MOST] = jnp.where(lane2 == spot, 1.0, 0.0).astype(BF)
    loads[2].wait()
    sent[...] = (
        jnp.dot(onehot[...], tokb[...], preferred_element_type=F32).astype(BF).reshape(N_EP, MOST, WID)
    )
    came[PAD] = sent[ep]
    came[:PAD] = jnp.zeros((PAD, MOST, WID), BF)
    result[...] = jnp.zeros_like(result)
    with jax.named_scope("barrier"):
        pl.semaphore_wait(barrier, len(peers))

    def send_to(ds):
        for i in range(1, N_EP):
            if min(PLACES[i][0], N_Z - PLACES[i][0]) in ds:
                e, peer = ep_peer(i)
                remote(sent.at[e], came.at[PAD + i], z_send.at[0], z_recv.at[stage_of(i)], peer).start()

    def tell(n, k):
        for steps in (n, N_Z - n):
            there = {"ep": lax.rem(ep + 2 * steps, N_EP), "tp": tp}
            pl.semaphore_signal(chain.at[k], inc=1, device_id=there, device_id_type=MESH)

    def told(k):
        with jax.named_scope("chain"):
            pl.semaphore_wait(chain.at[k], 2)

    tell(1, 0)
    send_to((0, 1))
    told(0)
    tell(2, 1)
    send_to((2,))
    told(1)
    tell(2, 2)
    tell(4, 3)
    send_to((3, 4))
    told(2)
    send_to((5, 6))
    told(3)
    send_to((7, 8))

    for q in range(N_EP * MOST // TOK):
        tall = []
        for e in range(q * PER, (q + 1) * PER):
            tall.append(jnp.where(lane1 == sel_t[:, e : e + 1], aff_t[:, e : e + 1], 0.0))
        wide = jnp.concatenate(tall, axis=0).T
        high = wide.astype(BF)
        mix[0, :, q * TOK : (q + 1) * TOK] = high
        mix[1, :, q * TOK : (q + 1) * TOK] = (wide - high.astype(F32)).astype(BF)

    lane_row = lax.broadcasted_iota(jnp.int32, (1, WID), 1)
    lane_slot = lax.rem(lane_row, MOST).astype(F32)
    lane_group = lane_row // MOST

    starts, counts = [], []
    total = jnp.zeros((1, WID), F32)
    gathers = {}

    def wait_for(block, semaphore):
        pltpu.make_async_copy(block, block, semaphore).wait()

    def span(c, half):
        n = (EDGES[c + 1] - EDGES[c]) // 2
        return pl.ds(EDGES[c] + half * n, n)

    def first_half(c):
        return pl.ds(0, (EDGES[c + 1] - EDGES[c]) // 2)

    def begin_gather(c):
        for i in (2, 1, 3):
            for half in (0, 1):
                block = rows.at[tp, span(c, half)]
                copy = remote(
                    block, block, a1_send.at[0], a1_recv.at[c, half, i], line(half, i)[1]
                )
                copy.start()
                gathers[c, half, i] = copy
        for i in (2, 1, 3):
            for half in (0, 1):
                block = rows.at[tp, span(c, half)]
                remote(block, block, a2_send.at[0], a2_recv.at[c], line(1 - half, i)[1]).start()

    def pick_rows(c):
        nonlocal total
        low, high = EDGES[c], EDGES[c + 1]
        before, known = len(counts), known_at(c)
        with jax.named_scope("zwait"):
            new = max(before, 1)
            wait_for(came.at[pl.ds(PAD + new, known - new)], z_recv.at[c])
        for j in range(before, known):
            live = jnp.where(came[PAD + j].astype(F32) < DEAD / 2, 1.0, 0.0)
            n = jnp.sum(live, axis=0, keepdims=True)
            counts.append(n)
            starts.append(total)
            total = total + n
        down_rows = lax.broadcasted_iota(jnp.int32, (high - low, WID), 0).astype(F32) + float(low)
        none = jnp.zeros((1, WID), F32)
        for t in range(TILES):
            first, many = none, none
            for k in range(PER):
                j = known - TILES * PER + t * PER + k
                first = jnp.where(lane_group == k, starts[j] if j >= 0 else none, first)
                many = jnp.where(lane_group == k, counts[j] if j >= 0 else none, many)
            place = jnp.where(lane_slot < many, first + lane_slot, -1.0)
            pick[: high - low, t * WID : (t + 1) * WID] = jnp.where(down_rows == place, 1.0, 0.0).astype(BF)
        block = came[PAD + known - TILES * PER : PAD + known].reshape(TILES * WID, WID)
        rows[tp, low:high] = jnp.dot(pick[: high - low], block, preferred_element_type=F32).astype(BF)
        begin_gather(c)

    def pass_on(c):
        for j in (1, 3, 2):
            for half in (0, 1):
                with jax.named_scope("pass_wait"):
                    gathers[c, half, j].wait_recv()
                source = line(half, SIDE - j)[0]
                block = rows.at[source, span(c, half)]
                for i in (2, 1, 3):
                    remote(block, block, a2_send.at[0], a2_recv.at[c], line(1 - half, i)[1]).start()

    def place_rows(_):
        down_slots = lax.broadcasted_iota(jnp.int32, (MOST, WID), 0).astype(F32)
        lanes = lax.broadcasted_iota(jnp.int32, (MOST, WID), 1).astype(F32)
        for j in range(N_EP):
            place = jnp.where(down_slots < counts[j], starts[j] + down_slots, -1.0)
            for q in range(ROWS // WID):
                spread[j * MOST : (j + 1) * MOST, q * WID : (q + 1) * WID] = jnp.where(
                    lanes + float(q * WID) == place, 1.0, 0.0
                ).astype(BF)

    def compute(c):
        with jax.named_scope("gather_wait"):
            wait_for(rows.at[pl.ds(0, N_TP - SIDE), pl.ds(EDGES[c], EDGES[c + 1] - EDGES[c])], a2_recv.at[c])
        if c == 0:
            for load in loads[3:]:
                load.wait()
        at = slice(EDGES[c], EDGES[c + 1])
        chosen = jnp.concatenate([rows[k, at] for k in range(N_TP)], axis=1)
        both = jnp.dot(chosen, wgu[...], preferred_element_type=F32)
        gate, up = both[:, :WID], both[:, WID:]
        hidden = (gate / (1.0 + jnp.exp(-gate)) * up).astype(BF)
        partial = jnp.dot(hidden, wdb[...], preferred_element_type=F32).astype(BF)
        for k in range(N_TP):
            part[k // SIDE, k % SIDE, at] = partial[:, k * WID : (k + 1) * WID]

    def begin_sum(c):
        for i in (2, 1, 3):
            for half in (0, 1):
                t, peer = line(half, i)
                if half == 0:
                    block = part.at[:, t % SIDE, span(c, half)]
                else:
                    block = part.at[t // SIDE, :, span(c, half)]
                there = got1.at[c, half, i - 1, :, first_half(c)]
                remote(block, there, r1_send.at[0], r1_recv.at[c, half], peer).start()

    def go_on_sum(c):
        for half in (0, 1):
            with jax.named_scope("sum1_wait"):
                wait_for(got1.at[c, half, :, :, first_half(c)], r1_recv.at[c, half])
            mine = part[:, x, span(c, half)] if half == 0 else part[y, :, span(c, half)]
            added = mine.astype(F32)
            for i in range(3):
                added = added + got1[c, half, i, :, first_half(c)].astype(F32)
            sum1[c, half, :, first_half(c)] = added.astype(BF)
            for i in (2, 1, 3):
                t, peer = line(1 - half, i)
                block = sum1.at[c, half, t // SIDE if half == 0 else t % SIDE, first_half(c)]
                remote(block, got2.at[c, half, i - 1, first_half(c)], r2_send.at[0], r2_recv.at[c], peer).start()

    done, left = set(), list(range(N_EP))

    def give_back(js):
        first, last = js[0], js[-1] + 1
        low = EDGES[chunks_of(first)[0]] // WID * WID
        high = -(-EDGES[chunks_of(js[-1])[-1] + 1] // WID) * WID
        slots = jnp.dot(
            spread[first * MOST : last * MOST, low:high],
            result[low:high],
            preferred_element_type=F32,
        ).astype(BF)
        back[first:last] = slots.reshape(last - first, MOST, WID)
        for i in reversed(js):
            if i == 0:
                home[ep] = back[0]
            else:
                remote(back.at[i], home.at[ep], b_send.at[0], b_recv.at[0], ep_back(i)[1]).start()

    def end_sum(c):
        with jax.named_scope("sum2_wait"):
            wait_for(got2.at[c, :, :, first_half(c)], r2_recv.at[c])
        for half in (0, 1):
            added = sum1[c, half, y if half == 0 else x, first_half(c)].astype(F32)
            for i in range(3):
                added = added + got2[c, half, i, first_half(c)].astype(F32)
            result[span(c, half)] = added.astype(BF)
        done.add(c)
        ready = [i for i in left if done.issuperset(chunks_of(i))]
        runs = []
        for i in ready:
            left.remove(i)
            if runs and runs[-1][-1] == i - 1:
                runs[-1].append(i)
            else:
                runs.append([i])
        for js in reversed(runs):
            give_back(js)

    steps = {
        "Z": pick_rows,
        "F": pass_on,
        "P": place_rows,
        "K": compute,
        "B": begin_sum,
        "S": go_on_sum,
        "E": end_sum,
    }
    for step in STEPS:
        steps[step[0]](int(step[1:] or 0))

    wait_for(sent.at[pl.ds(1, N_EP - 1)], z_send.at[0])
    wait_for(rows.at[pl.ds(0, 3)], a1_send.at[0])
    wait_for(rows.at[pl.ds(0, 12)], a2_send.at[0])
    wait_for(rows.at[pl.ds(0, 12)], r1_send.at[0])
    wait_for(rows.at[pl.ds(0, 3)], r2_send.at[0])
    wait_for(back.at[pl.ds(1, N_EP - 1)], b_send.at[0])
    with jax.named_scope("home_wait"):
        wait_for(home.at[pl.ds(1, N_EP - 1)], b_recv.at[0])
    slots = home[...].reshape(N_EP * MOST, WID)
    out[...] = (
        jnp.dot(mix[0], slots, preferred_element_type=F32) + jnp.dot(mix[1], slots, preferred_element_type=F32)
    ).astype(BF)


def per_device(tokens, selected, affinity, w_gate, w_up, w_down):
    width = tokens.shape[1]
    dma = pltpu.SemaphoreType.DMA
    scratch = [
        pltpu.VMEM((2 * TOK, WID), BF),
        pltpu.VMEM((N_EP, MOST), jnp.int32),
        pltpu.VMEM((N_EP, MOST), F32),
        pltpu.VMEM((width, 2 * WID), BF),
        pltpu.VMEM((WID, width), BF),
        pltpu.VMEM((N_EP * MOST, 2 * TOK), BF),
        pltpu.VMEM((N_EP, MOST, WID), BF),
        pltpu.VMEM((PAD + N_EP, MOST, WID), BF),
        pltpu.VMEM((LARGEST, TILES * WID), BF),
        pltpu.VMEM((N_EP * MOST, ROWS), BF),
        pltpu.VMEM((N_TP, ROWS, WID), BF),
        pltpu.VMEM((SIDE, SIDE, ROWS, WID), BF),
        pltpu.VMEM((CHUNKS, 2, 3, SIDE, LARGEST // 2, WID), BF),
        pltpu.VMEM((CHUNKS, 2, SIDE, LARGEST // 2, WID), BF),
        pltpu.VMEM((CHUNKS, 2, 3, LARGEST // 2, WID), BF),
        pltpu.VMEM((ROWS, WID), BF),
        pltpu.VMEM((N_EP, MOST, WID), BF),
        pltpu.VMEM((N_EP, MOST, WID), BF),
        pltpu.VMEM((2, TOK, N_EP * MOST), BF),
        pltpu.SemaphoreType.REGULAR((4,)),
        dma((6,)),
        dma((1,)),
        dma((CHUNKS,)),
        dma((1,)),
        dma((CHUNKS, 2, 4)),
        dma((1,)),
        dma((CHUNKS,)),
        dma((1,)),
        dma((CHUNKS, 2)),
        dma((1,)),
        dma((CHUNKS,)),
        dma((1,)),
        dma((1,)),
    ]
    return pl.pallas_call(
        kernel,
        out_shape=jax.ShapeDtypeStruct((tokens.shape[0], WID), BF),
        in_specs=[pl.BlockSpec(memory_space=pl.ANY)] * 6,
        out_specs=pl.BlockSpec(memory_space=pltpu.VMEM),
        scratch_shapes=scratch,
        compiler_params=pltpu.CompilerParams(
            collective_id=0, has_side_effects=True, vmem_limit_bytes=67043328
        ),
    )(tokens, selected, affinity, w_gate[0], w_up[0], w_down[0])


def solution(mesh):
    return jax.shard_map(
        per_device,
        mesh=mesh,
        in_specs=(
            P("ep", None),
            P(None, "ep"),
            P(None, "ep"),
            P("ep", None, "tp"),
            P("ep", None, "tp"),
            P("ep", "tp", None),
        ),
        out_specs=P("ep", "tp"),
        check_vma=False,
    )
```

time: 87.8 us -> 73.5 us (0.84)
  Pallas kernels: 81.2 us -> 71.9 us
  local copies, waits for them, and re-layouts: 6.22 us -> 1.38 us
    pallas_call x1, Pallas kernels: 81.2 us -> 71.9 us  [per_device(): pl.pallas_call(kernel, out_shape=jax.ShapeDtypeStruct((tokens.shape[0], W...]
    unnamed x13 -> x1, local copies, waits for them, and re-layouts: 6.22 us -> 1.38 us
where the time goes in v2:
time: 73.5 us; the launch traced here: 73.3 us
  Pallas kernels  71.9 us (98%)
  local copies, waits for them, and re-layouts  1.38 us (2%)
    pallas_call x1, Pallas kernels, per_device(): pl.pallas_call(kernel, out_shape=jax.ShapeDtypeStruct((tokens.shape[0], W...  71.9 us

profile of v2, /device:TPU:1, one launch (start us, length us, event | category | flops | bytes accessed | tf_op | source)
XLA Modules:
  0.0 73.3 jit_solution(9334714062147550259)
XLA Ops:
  0.0 71.9 %shard_map.64 = bf16[128,128]{1,0:T(8,128)(2,1)} custom-call(bf16[128,2048]{1,0:T(8,128)(2,1)} %tok.1, s32[32,32]{1,0:T(8,128)} %sel.1, f32[32,32]{1,0:T(8,128)} %aff.1, bf16[2048,128]{1,0:T(8,128)(2,1)} %bitcast.3, bf16[2048,128]{1,0:T(8,128)(2,1)} %bitcast.4, bf16[128,2048]{1,0:T(8,128)(2,1)} %bitcast.5), custom_call_target="tpu_custom_call" | custom-call | tf_op jit(solution)/shard_map/pallas_call | solution.py:377
  71.9 1.4 %copy.8 = bf16[128,128]{1,0:T(8,128)(2,1)} copy(bf16[128,128]{1,0:T(8,128)(2,1)} %shard_map.64) | data formatting | bytes 65536

commit v3 on v2

--- a/solution.py
+++ b/solution.py
@@ -16,11 +16,11 @@
 ROWS = 512
 EDGES = (0, 64, 192, 320, 448, 512)
 CHUNKS = len(EDGES) - 1
-LARGEST = 128
+LARGEST = max(b - a for a, b in zip(EDGES, EDGES[1:]))
 PER = WID // MOST
 FULL = ROWS // MOST
-TILES = 5
-PAD = 2
+TILES = -(-(LARGEST // MOST + FULL) // PER)
+PAD = max(0, TILES * PER - (N_EP - FULL + EDGES[1] // MOST))
 DEAD = 1024.0
 
 PLACES = [(0, 0), (0, 1)]
@@ -89,14 +89,27 @@
     for load in loads:
         load.start()
     barrier = pltpu.get_barrier_semaphore()
-    peers = [ep_peer(i)[1] for i in range(1, 6)]
+    peers = [ep_peer(i)[1] for i in range(1, 10)]
     peers += [line(a, i)[1] for a in (0, 1) for i in (1, 2, 3)]
     for peer in peers:
         pl.semaphore_signal(barrier, inc=1, device_id=peer, device_id_type=MESH)
 
     tokb[TOK : 2 * TOK] = jnp.full((TOK, WID), DEAD, BF)
-    loads[0].wait()
-    loads[1].wait()
+    for load in loads[:3]:
+        load.wait()
+    with jax.named_scope("barrier"):
+        pl.semaphore_wait(barrier, len(peers))
+
+    def tell(n, k):
+        for steps in (n, N_Z - n):
+            there = {"ep": lax.rem(ep + 2 * steps, N_EP), "tp": tp}
+            pl.semaphore_signal(chain.at[k], inc=1, device_id=there, device_id_type=MESH)
+
+    def told(k):
+        with jax.named_scope("chain"):
+            pl.semaphore_wait(chain.at[k], 2)
+
+    tell(2, 0)
     sel_t = selb[...].astype(F32).T
     aff_t = affb[...].T
     lane2 = lax.broadcasted_iota(jnp.int32, (MOST, 2 * TOK), 1).astype(F32)
@@ -105,15 +118,9 @@
         column = sel_t[:, e : e + 1]
         spot = jnp.where(column < 0.0, float(TOK), column)
         onehot[e * MOST : (e + 1) * MOST] = jnp.where(lane2 == spot, 1.0, 0.0).astype(BF)
-    loads[2].wait()
     sent[...] = (
         jnp.dot(onehot[...], tokb[...], preferred_element_type=F32).astype(BF).reshape(N_EP, MOST, WID)
     )
-    came[PAD] = sent[ep]
-    came[:PAD] = jnp.zeros((PAD, MOST, WID), BF)
-    result[...] = jnp.zeros_like(result)
-    with jax.named_scope("barrier"):
-        pl.semaphore_wait(barrier, len(peers))
 
     def send_to(ds):
         for i in range(1, N_EP):
@@ -121,28 +128,19 @@
                 e, peer = ep_peer(i)
                 remote(sent.at[e], came.at[PAD + i], z_send.at[0], z_recv.at[stage_of(i)], peer).start()
 
-    def tell(n, k):
-        for steps in (n, N_Z - n):
-            there = {"ep": lax.rem(ep + 2 * steps, N_EP), "tp": tp}
-            pl.semaphore_signal(chain.at[k], inc=1, device_id=there, device_id_type=MESH)
-
-    def told(k):
-        with jax.named_scope("chain"):
-            pl.semaphore_wait(chain.at[k], 2)
-
-    tell(1, 0)
-    send_to((0, 1))
+    send_to((0, 1, 2))
     told(0)
     tell(2, 1)
-    send_to((2,))
+    tell(4, 2)
+    send_to((3, 4))
     told(1)
-    tell(2, 2)
-    tell(4, 3)
-    send_to((3, 4))
+    send_to((5, 6))
     told(2)
-    send_to((5, 6))
-    told(3)
     send_to((7, 8))
+    came[PAD] = sent[ep]
+    if PAD:
+        came[:PAD] = jnp.zeros((PAD, MOST, WID), BF)
+    result[...] = jnp.zeros_like(result)
 
     for q in range(N_EP * MOST // TOK):
         tall = []
@@ -150,8 +148,8 @@
             tall.append(jnp.where(lane1 == sel_t[:, e : e + 1], aff_t[:, e : e + 1], 0.0))
         wide = jnp.concatenate(tall, axis=0).T
         high = wide.astype(BF)
-        mix[0, :, q * TOK : (q + 1) * TOK] = high
-        mix[1, :, q * TOK : (q + 1) * TOK] = (wide - high.astype(F32)).astype(BF)
+        mix[:TOK, q * TOK : (q + 1) * TOK] = high
+        mix[TOK:, q * TOK : (q + 1) * TOK] = (wide - high.astype(F32)).astype(BF)
 
     lane_row = lax.broadcasted_iota(jnp.int32, (1, WID), 1)
     lane_slot = lax.rem(lane_row, MOST).astype(F32)
@@ -303,7 +301,7 @@
         runs = []
         for i in ready:
             left.remove(i)
-            if runs and runs[-1][-1] == i - 1:
+            if runs and runs[-1][-1] == i - 1 and len(runs[-1]) < MOST // 4:
                 runs[-1].append(i)
             else:
                 runs.append([i])
@@ -331,9 +329,8 @@
     with jax.named_scope("home_wait"):
         wait_for(home.at[pl.ds(1, N_EP - 1)], b_recv.at[0])
     slots = home[...].reshape(N_EP * MOST, WID)
-    out[...] = (
-        jnp.dot(mix[0], slots, preferred_element_type=F32) + jnp.dot(mix[1], slots, preferred_element_type=F32)
-    ).astype(BF)
+    weighted = jnp.dot(mix[...], slots, preferred_element_type=F32)
+    out[...] = (weighted[:TOK] + weighted[TOK:]).astype(BF)
 
 
 def per_device(tokens, selected, affinity, w_gate, w_up, w_down):
@@ -358,8 +355,8 @@
         pltpu.VMEM((ROWS, WID), BF),
         pltpu.VMEM((N_EP, MOST, WID), BF),
         pltpu.VMEM((N_EP, MOST, WID), BF),
-        pltpu.VMEM((2, TOK, N_EP * MOST), BF),
-        pltpu.SemaphoreType.REGULAR((4,)),
+        pltpu.VMEM((2 * TOK, N_EP * MOST), BF),
+        pltpu.SemaphoreType.REGULAR((3,)),
         dma((6,)),
         dma((1,)),
         dma((CHUNKS,)),

time: 73.5 us -> 72.8 us (level)
  no operation moved by 1% of the time
where the time goes in v3:
time: 72.8 us; the launch traced here: 72.6 us
  Pallas kernels  71.2 us (98%)
  local copies, waits for them, and re-layouts  1.38 us (2%)
    pallas_call x1, Pallas kernels, per_device(): pl.pallas_call(kernel, out_shape=jax.ShapeDtypeStruct((tokens.shape[0], W...  71.2 us

profile of v3, /device:TPU:1, one launch (start us, length us, event | category | flops | bytes accessed | tf_op | source)
XLA Modules:
  0.0 72.6 jit_solution(2189332539024767813)
XLA Ops:
  0.0 71.2 %shard_map.64 = bf16[128,128]{1,0:T(8,128)(2,1)} custom-call(bf16[128,2048]{1,0:T(8,128)(2,1)} %tok.1, s32[32,32]{1,0:T(8,128)} %sel.1, f32[32,32]{1,0:T(8,128)} %aff.1, bf16[2048,128]{1,0:T(8,128)(2,1)} %bitcast.3, bf16[2048,128]{1,0:T(8,128)(2,1)} %bitcast.4, bf16[128,2048]{1,0:T(8,128)(2,1)} %bitcast.5), custom_call_target="tpu_custom_call" | custom-call | tf_op jit(solution)/shard_map/pallas_call | solution.py:374
  71.2 1.4 %copy.8 = bf16[128,128]{1,0:T(8,128)(2,1)} copy(bf16[128,128]{1,0:T(8,128)(2,1)} %shard_map.64) | data formatting | bytes 65536

commit v4 on v3

--- a/solution.py
+++ b/solution.py
@@ -14,7 +14,7 @@
 N_EP, N_TP, N_Z, SIDE = 32, 16, 16, 4
 MOST, TOK, WID = 32, 128, 128
 ROWS = 512
-EDGES = (0, 64, 192, 320, 448, 512)
+EDGES = (0, 64, 160, 288, 416, 512)
 CHUNKS = len(EDGES) - 1
 LARGEST = max(b - a for a, b in zip(EDGES, EDGES[1:]))
 PER = WID // MOST

time: 72.8 us -> 71.8 us (0.986)
  Pallas kernels: 71.2 us -> 70.2 us
    pallas_call x1, Pallas kernels: 71.2 us -> 70.2 us  [per_device(): pl.pallas_call(kernel, out_shape=jax.ShapeDtypeStruct((tokens.shape[0], W...]
where the time goes in v4:
time: 71.8 us; the launch traced here: 71.6 us
  Pallas kernels  70.2 us (98%)
  local copies, waits for them, and re-layouts  1.38 us (2%)
    pallas_call x1, Pallas kernels, per_device(): pl.pallas_call(kernel, out_shape=jax.ShapeDtypeStruct((tokens.shape[0], W...  70.2 us

profile of v4, /device:TPU:1, one launch (start us, length us, event | category | flops | bytes accessed | tf_op | source)
XLA Modules:
  0.0 71.6 jit_solution(6328372639495100300)
XLA Ops:
  0.0 70.2 %shard_map.64 = bf16[128,128]{1,0:T(8,128)(2,1)} custom-call(bf16[128,2048]{1,0:T(8,128)(2,1)} %tok.1, s32[32,32]{1,0:T(8,128)} %sel.1, f32[32,32]{1,0:T(8,128)} %aff.1, bf16[2048,128]{1,0:T(8,128)(2,1)} %bitcast.3, bf16[2048,128]{1,0:T(8,128)(2,1)} %bitcast.4, bf16[128,2048]{1,0:T(8,128)(2,1)} %bitcast.5), custom_call_target="tpu_custom_call" | custom-call | tf_op jit(solution)/shard_map/pallas_call | solution.py:374
  70.2 1.4 %copy.8 = bf16[128,128]{1,0:T(8,128)(2,1)} copy(bf16[128,128]{1,0:T(8,128)(2,1)} %shard_map.64) | data formatting | bytes 65536
